TPU v7x, 32 devices: a whole 2x2x4 slice. The times are simulated.
32 devices in a mesh: ep: 16 (over z, y, x), tp: 2 (over core).
Axes of the slice: x: 2, y: 2, z: 4, core: 2. Of those that a mesh axis runs over, the one named last changes fastest.
Arguments:
- tokens: bfloat16 [384, 2048], P('ep'), may hold values from -40 to 40
- old_state: float32 [384, 16, 4096], P('ep', 'tp'), may hold values from -6 to 6
- w_query: bfloat16 [2048, 1024], P(None, 'tp'), may hold values from -0.125 to 0.125
- w_forget: bfloat16 [2048, 1024], P(None, 'tp'), may hold values from -0.125 to 0.125
- w_value: bfloat16 [2048, 1024], P(None, 'tp'), may hold values from -0.125 to 0.125
- w_gate: bfloat16 [2048, 1024], P(None, 'tp'), may hold values from -0.125 to 0.125
- lower_bound: float32 [1024], P('tp'), may hold values from 0.05 to 0.9
- head_gain: float32 [64], replicated, may hold values from 0.1 to 1.9
- w_out: bfloat16 [1024, 2048], P('tp'), may hold values from -0.1875 to 0.1875
- mix_gain: float32 [2048], replicated, may hold values from 0.1 to 1.9
- expert_gate: bfloat16 [16, 2048, 512], P('ep', None, 'tp'), may hold values from -0.125 to 0.125
- expert_up: bfloat16 [16, 2048, 512], P('ep', None, 'tp'), may hold values from -0.125 to 0.125
- expert_down: bfloat16 [16, 512, 2048], P('ep', 'tp'), may hold values from -0.25 to 0.25
- expert_ids: int32 [384, 2], P('ep'), may hold values from 0 to 15, as said below
- route_weight: float32 [384, 2], P('ep'), may hold values from 0.1 to 1
- moe_gain: float32 [2048], replicated, may hold values from 0.1 to 1.9
Outputs:
- next_tokens: bfloat16 [384, 2048], P('ep', 'tp')
- new_state: float32 [384, 16, 4096], P('ep', 'tp')
Inputs may be any that keep to these rules, and one draw needn't show every extreme that they name: `expert_ids`: each row names two different experts of one group of 4 consecutive experts. In each aligned block of 24 rows no expert is named by more than 6 rows, and one expert, the same in every block, is named by exactly 6 rows of every block.
All inputs are finite; a program needn't handle non-finite values.
Results may differ from a plain program's by a relative error of at most 0.011.
Values may be sent and summed in bfloat16 or wider, within the bound.
A program may use at most 128 MiB of HBM per device.

v0:
```python
import jax
import jax.numpy as jnp
from jax import lax
from jax.sharding import PartitionSpec as P


def layer_normed(values, gain):
    center = jnp.mean(values, -1, keepdims=True)
    centered = values - center
    variance = jnp.mean(centered * centered, -1, keepdims=True)
    return centered * lax.rsqrt(variance + 1e-05) * gain


def rounded(values):
    return lax.optimization_barrier(values.astype(jnp.bfloat16)).astype(jnp.float32)


def slot_table(ids_block, expert_count, capacity):
    flat_ids = ids_block.reshape(-1)
    onehot = (flat_ids[:, None] == jnp.arange(expert_count, dtype=jnp.int32)[None, :]).astype(
        jnp.int32
    )
    before = jnp.cumsum(onehot, 0) - onehot
    rank = jnp.sum(before * onehot, 1)
    return flat_ids * capacity + rank


def per_device(
    tokens,
    old_state,
    w_query,
    w_forget,
    w_value,
    w_gate,
    lower_bound,
    head_gain,
    w_out,
    mix_gain,
    expert_gate,
    expert_up,
    expert_down,
    expert_ids,
    route_weight,
    moe_gain,
):
    row_count, model_width = tokens.shape
    heads_here = old_state.shape[1]
    head_dim = head_gain.shape[0]
    head_cols = w_query.shape[1]
    q_lin = jnp.dot(tokens, w_query, preferred_element_type=jnp.float32)
    f_lin = jnp.dot(tokens, w_forget, preferred_element_type=jnp.float32)
    v_lin = jnp.dot(tokens, w_value, preferred_element_type=jnp.float32)
    g_lin = jnp.dot(tokens, w_gate, preferred_element_type=jnp.float32)
    act_query = jax.nn.silu(q_lin).reshape(row_count, heads_here, head_dim)
    bound = lower_bound.reshape(heads_here, head_dim)
    forget = bound + (1.0 - bound) * jax.nn.sigmoid(f_lin.reshape(row_count, heads_here, head_dim))
    previous = old_state.reshape(row_count, heads_here, head_dim, head_dim)
    new_state = forget[..., None] * previous + (1.0 - forget)[..., None] * v_lin.reshape(
        row_count, heads_here, 1, head_dim
    )
    readout = jnp.einsum("shi,shij->shj", act_query, new_state, precision=lax.Precision.HIGHEST)
    normed = readout * lax.rsqrt(jnp.mean(readout * readout, -1, keepdims=True) + 1e-06) * head_gain
    mixer_out = (
        (normed * jax.nn.silu(g_lin.reshape(row_count, heads_here, head_dim)))
        .reshape(row_count, head_cols)
        .astype(jnp.bfloat16)
    )
    own_part = rounded(jnp.dot(mixer_out, w_out, preferred_element_type=jnp.float32))
    mixed = lax.psum(own_part.astype(jnp.bfloat16), "tp").astype(jnp.float32)
    after_mixer = layer_normed(tokens.astype(jnp.float32) + mixed, mix_gain).astype(jnp.bfloat16)
    expert_count = lax.axis_size("ep")
    core_count = lax.axis_size("tp")
    top_count = expert_ids.shape[1]
    capacity = max(2, 2 * top_count * row_count // expert_count)
    slot_ids = slot_table(expert_ids, expert_count, capacity)
    choose = (
        slot_ids[None, :] == jnp.arange(expert_count * capacity, dtype=jnp.int32)[:, None]
    ).astype(jnp.bfloat16)
    choose = choose.reshape(expert_count * capacity, row_count, top_count).sum(-1)
    outgoing = jnp.dot(choose, after_mixer, preferred_element_type=jnp.float32).astype(jnp.bfloat16)
    outgoing = outgoing.reshape(expert_count, capacity, model_width)
    arrived = lax.all_to_all(outgoing, "ep", split_axis=0, concat_axis=0, tiled=True)
    sources = arrived.shape[0]
    slots_now = arrived.shape[1]
    rows_in = arrived.reshape(sources * slots_now, model_width)
    gate_act = jnp.dot(rows_in, expert_gate[0], preferred_element_type=jnp.float32)
    up_act = jnp.dot(rows_in, expert_up[0], preferred_element_type=jnp.float32)
    hidden = (jax.nn.silu(gate_act) * up_act).astype(jnp.bfloat16)
    partial_rows = rounded(jnp.dot(hidden, expert_down[0], preferred_element_type=jnp.float32))
    summed_rows = lax.psum_scatter(
        partial_rows.astype(jnp.bfloat16), "tp", scatter_dimension=1, tiled=True
    ).astype(jnp.float32)
    results = summed_rows.astype(jnp.bfloat16).reshape(sources, slots_now, summed_rows.shape[1])
    back_half = lax.all_to_all(results, "ep", split_axis=0, concat_axis=0, tiled=True)
    returned = lax.all_gather(back_half, "tp", axis=2, tiled=True)
    flat_back = returned.reshape(expert_count * capacity, model_width)
    picked = (
        jnp.take(flat_back, slot_ids, axis=0)
        .reshape(row_count, top_count, model_width)
        .astype(jnp.float32)
    )
    moe_sum = jnp.sum(picked * route_weight[..., None], 1)
    full_rows = layer_normed(after_mixer.astype(jnp.float32) + moe_sum, moe_gain).astype(
        jnp.bfloat16
    )
    half_width = model_width // core_count
    next_tokens = lax.dynamic_slice_in_dim(
        full_rows, lax.axis_index("tp") * half_width, half_width, 1
    )
    return (next_tokens, new_state.reshape(row_count, heads_here, head_dim * head_dim))


def solution(mesh):
    in_specs = (
        P("ep", None),
        P("ep", "tp", None),
        P(None, "tp"),
        P(None, "tp"),
        P(None, "tp"),
        P(None, "tp"),
        P("tp"),
        P(),
        P("tp", None),
        P(),
        P("ep", None, "tp"),
        P("ep", None, "tp"),
        P("ep", "tp", None),
        P("ep", None),
        P("ep", None),
        P(),
    )
    out_specs = (P("ep", "tp"), P("ep", "tp", None))
    return jax.shard_map(
        per_device, mesh=mesh, in_specs=in_specs, out_specs=out_specs, check_vma=False
    )
```

profile of v0, /device:TPU:0, one launch (start us, length us, event | category | flops | bytes accessed | tf_op | source)
XLA Modules:
  0.0 128.8 jit_solution(17914694816942390285)
XLA Ops:
  7.2 0.9 add.128
  8.1 2.1 %fusion.7 = f32[24,512]{1,0:T(8,128)S(1)} fusion(bf16[24,2048]{1,0:T(8,128)(2,1)} %param.16, bf16[2048,512]{1,0:T(8,128)(2,1)} %param.19), kind=kOutput, calls=%fused_computation.15 | convolution fusion | flops 50368512 | bytes 2244608 | tf_op jit(solution)/shard_map/dot_general | solution.py:51
  10.3 2.0 %fusion.33 = f32[24,512]{1,0:T(8,128)S(1)} fusion(bf16[24,2048]{1,0:T(8,128)(2,1)} %param.16, bf16[2048,512]{1,0:T(8,128)(2,1)} %param.20), kind=kOutput, calls=%fused_computation.66 | convolution fusion | flops 50331648 | bytes 2244608 | tf_op jit(solution)/shard_map/dot_general | solution.py:52
  12.3 0.1 mul.165
  12.4 6.1 %reshape.162 = f32[24,8,64,64]{3,2,1,0:T(8,128)} reshape(f32[24,8,4096]{2,1,0:T(8,128)} %param.17) | data formatting | bytes 6291456 | tf_op jit(solution)/shard_map/reshape | solution.py:57
  18.5 2.0 %divide_multiply_fusion = f32[24,512]{1,0:T(8,128)S(1)} fusion(bf16[24,2048]{1,0:T(8,128)(2,1)S(1)} %copy-done.1, bf16[2048,512]{1,0:T(8,128)(2,1)} %param.18), kind=kOutput, calls=%fused_computation.44 | convolution fusion | flops 50380800 | bytes 2244608 | tf_op jit(solution)/shard_map/dot_general | solution.py:50
  20.7 9.6 %fusion = f32[24,8,1,64]{3,2,1,0:T(1,128)S(1)} fusion(f32[24,8,64,1]{2,3,1,0:T(1,128)S(1)} %bitcast.40, f32[24,8,64,64]{3,2,1,0:T(8,128)} %reshape.162, f32[24,8,64]{2,1,0:T(8,128)S(1)} %get-tuple-element.7, f32[24,8,64]{2,1,0:T(8,128)S(1)} %mul.165, f32[24,8,64]{2,1,0:T(8,128)S(1)} %get-tuple-element.6), kind=kOutput, calls=%fused_computation.1 | convolution fusion | flops 11796480 | bytes 3391488 | tf_op jit(solution)/shard_map/shi,shij->shj/dot_general | solution.py:61
  30.3 0.1 multiply_reduce_fusion.3
  30.4 0.4 fusion.34
  30.8 0.1 reshape.163
  30.9 0.1 multiply_convert_fusion.1
  31.0 0.1 convert_element_type.53
  31.1 1.0 convolution_convert_fusion.2
  32.2 0.1 copy.28
  32.3 0.1 reshape.164
  32.6 0.2 select_reduce_fusion
  32.7 0.1 reduce_sum.83
  33.0 19.9 %all-reduce.2.cloned.1.call-done = bf16[24,2048]{1,0:T(8,128)(2,1)} async-done(((bf16[24,2048]{1,0:T(8,128)(2,1)}), bf16[24,2048]{1,0:T(8,128)(2,1)}) %all-reduce.2.cloned.1.call-update) | async-done | bytes 98320 | tf_op jit(solution)/shard_map/psum | solution.py:69
  52.9 1.0 fusion.14
  53.9 1.1 multiply_reduce_fusion.2
  55.1 1.0 multiply_convert_fusion
  56.1 0.3 convolution_convert_fusion.1
  56.4 0.9 reshape.165
  57.3 6.8 %all-to-all-start = ((bf16[16,6,2048]{2,1,0:T(8,128)(2,1)}), bf16[16,6,2048]{2,1,0:T(8,128)(2,1)S(1)}, u32[]{:S(2)}, u32[]{:S(2)}) async-start(bf16[16,6,2048]{2,1,0:T(8,128)(2,1)} %reshape.165), calls=%async_computation | async-start | bytes 1048576 | tf_op jit(solution)/shard_map/all_to_all | solution.py:82
  64.2 3.8 %broadcast_multiply_fusion = f32[24,8,64,64]{3,2,1,0:T(8,128)} fusion(f32[24,8,64]{2,1,0:T(8,128)S(1)} %mul.165, f32[24,8,64]{2,1,0:T(8,128)S(1)} %get-tuple-element.6), kind=kLoop, calls=%fused_computation.5 | loop fusion | flops 786432 | bytes 3244032 | tf_op jit(solution)/shard_map/mul | solution.py:58
  68.0 5.8 %mul.196 = f32[24,8,4096]{2,1,0:T(8,128)} reshape(f32[24,8,64,64]{3,2,1,0:T(8,128)} %broadcast_multiply_fusion) | data formatting | bytes 6291456 | tf_op jit(solution)/shard_map/mul | solution.py:58
  73.8 3.8 %mul.162 = f32[24,8,64,64]{3,2,1,0:T(8,128)} broadcast(f32[24,8,64]{2,1,0:T(8,128)S(1)} %get-tuple-element.7), dimensions={0,1,2} | broadcast | bytes 3194880 | tf_op jit(solution)/shard_map/mul | solution.py:58
  77.6 5.9 %mul.194 = f32[24,8,4096]{2,1,0:T(8,128)} reshape(f32[24,8,64,64]{3,2,1,0:T(8,128)} %mul.162) | data formatting | bytes 6291456 | tf_op jit(solution)/shard_map/mul | solution.py:58
  83.5 0.1 reshape.166
  83.7 1.5 %fusion.11 = f32[96,256]{1,0:T(8,128)S(1)} fusion(bf16[96,2048]{1,0:T(8,128)(2,1)S(1)} %reshape.166, bf16[1,2048,256]{2,1,0:T(8,128)(2,1)} %param.26), kind=kOutput, calls=%fused_computation.18 | convolution fusion | flops 100663296 | bytes 1540096 | tf_op jit(solution)/shard_map/dot_general | solution.py:86
  85.2 3.1 %convolution_convert_fusion = bf16[96,2048]{1,0:T(8,128)(2,1)} fusion(bf16[96,2048]{1,0:T(8,128)(2,1)S(1)} %reshape.166, bf16[1,256,2048]{2,1,0:T(8,128)(2,1)} %param.28, bf16[1,2048,256]{2,1,0:T(8,128)(2,1)} %param.27, f32[96,256]{1,0:T(8,128)S(1)} %fusion.11), kind=kOutput, calls=%fused_computation.7 | convolution fusion | flops 201670656 | bytes 2981888 | tf_op jit(solution)/shard_map/dot_general | solution.py:89
  88.3 6.2 %multiply_add_fusion = f32[24,8,4096]{2,1,0:T(8,128)} fusion(f32[24,8,4096]{2,1,0:T(8,128)} %mul.196, f32[24,8,4096]{2,1,0:T(8,128)} %mul.194, f32[24,8,4096]{2,1,0:T(8,128)} %param.17), kind=kLoop, calls=%fused_computation.4 | loop fusion | flops 1572864 | bytes 12582912 | tf_op jit(solution)/shard_map/add | solution.py:58
  94.5 3.1 %reduce-scatter.2.cloned.1.call-done = bf16[96,1024]{1,0:T(8,128)(2,1)} async-done(((bf16[96,2048]{1,0:T(8,128)(2,1)}), bf16[96,1024]{1,0:T(8,128)(2,1)}) %reduce-scatter.2.cloned.1.call-update) | async-done | bytes 196624 | tf_op jit(solution)/shard_map/reduce_scatter | solution.py:90
  97.5 1.7 %reshape.167 = bf16[16,6,1024]{2,1,0:T(8,128)(2,1)} reshape(bf16[96,1024]{1,0:T(8,128)(2,1)} %reduce-scatter.2.cloned.1.call-done) | data formatting | bytes 393216 | tf_op jit(solution)/shard_map/reshape | solution.py:93
  99.2 6.7 %all-to-all-start.1 = ((bf16[16,6,1024]{2,1,0:T(8,128)(2,1)}), bf16[16,6,1024]{2,1,0:T(8,128)(2,1)S(1)}, u32[]{:S(2)}, u32[]{:S(2)}) async-start(bf16[16,6,1024]{2,1,0:T(8,128)(2,1)} %reshape.167), calls=%async_computation.2 | async-start | bytes 524288 | tf_op jit(solution)/shard_map/all_to_all | solution.py:94
  106.0 0.1 copy.31
  106.1 0.1 mul.185
  106.2 0.1 copy.30
  106.3 0.1 copy.32
  106.4 10.0 %all-to-all-done.1 = bf16[16,6,1024]{2,1,0:T(8,128)(2,1)S(1)} async-done(((bf16[16,6,1024]{2,1,0:T(8,128)(2,1)}), bf16[16,6,1024]{2,1,0:T(8,128)(2,1)S(1)}, u32[]{:S(2)}, u32[]{:S(2)}) %all-to-all-start.1) | async-done | bytes 196640 | tf_op jit(solution)/shard_map/all_to_all | solution.py:94
  116.4 2.2 %all_gather.3 = bf16[16,6,2048]{2,1,0:T(8,128)(2,1)S(1)} all-gather(bf16[16,6,1024]{2,1,0:T(8,128)(2,1)S(1)} %all-to-all-done.1), channel_id=1, replica_groups=mesh['ep'=16,'tp'=2] {'tp'}, dimensions={2}, use_global_device_ids=true | all-gather | bytes 589824 | tf_op jit(solution)/shard_map/all_gather | solution.py:95
  118.5 0.1 reshape.168
  118.7 0.7 gather_fusion
  119.4 0.1 gather.7
  119.5 1.4 %multiply_reduce_fusion = f32[24,2048]{1,0:T(8,128)S(1)} fusion(bf16[24,2,2048]{2,1,0:T(2,128)(2,1)S(1)} %gather.7, pred[24,2]{1,0:T(8,128)(4,1)S(1)} %copy.30, f32[24,2]{1,0:T(8,128)S(1)} %copy.32), kind=kLoop, calls=%fused_computation.20 | loop fusion | flops 344064 | bytes 393456 | tf_op jit(solution)/shard_map/reduce_sum | solution.py:102
  120.9 0.1 fusion.16
  121.1 0.2 multiply_reduce_fusion.1
  121.3 0.7 fusion.18
  (38 shorter events, 0.7 us)
Async XLA Ops:
  7.2 24.0 %copy-start = (bf16[512,2048]{1,0:T(8,128)(2,1)S(1)}, bf16[512,2048]{1,0:T(8,128)(2,1)}, u32[]{:S(2)}) copy-start(bf16[512,2048]{1,0:T(8,128)(2,1)} %param.24) | copy-start | bytes 6291460
  7.2 45.7 %all-reduce.2.cloned.1.call-start = ((), (), s32[]{:S(2)}) async-start(), calls=%async_computation.3 | async-start | bytes 196608 | tf_op jit(solution)/shard_map/psum | solution.py:69
  12.4 6.1 %copy-start.1 = (bf16[24,2048]{1,0:T(8,128)(2,1)S(1)}, bf16[24,2048]{1,0:T(8,128)(2,1)}, u32[]{:S(2)}) copy-start(bf16[24,2048]{1,0:T(8,128)(2,1)} %param.16) | copy-start | bytes 294916
  20.6 9.8 %copy-start.2 = (bf16[2048,512]{1,0:T(8,128)(2,1)S(1)}, bf16[2048,512]{1,0:T(8,128)(2,1)}, u32[]{:S(2)}) copy-start(bf16[2048,512]{1,0:T(8,128)(2,1)} %param.21) | copy-start | bytes 6291460
  20.7 10.3 %copy-start.6 = (f32[64]{0:T(128)S(1)}, f32[64]{0:T(128)}, u32[]{:S(2)}) copy-start(f32[64]{0:T(128)} %param.23) | copy-start | bytes 772
  30.3 1.9 %copy-start.3 = (s32[24,2]{0,1:T(2,128)S(1)}, s32[24,2]{0,1:T(2,128)}, u32[]{:S(2)}) copy-start(s32[24,2]{0,1:T(2,128)} %param.29) | copy-start | bytes 580
  30.3 24.8 %copy-start.4 = (f32[2048]{0:T(1024)S(1)}, f32[2048]{0:T(1024)}, u32[]{:S(2)}) copy-start(f32[2048]{0:T(1024)} %param.25) | copy-start | bytes 24580
  57.3 26.2 %all-to-all-start = ((bf16[16,6,2048]{2,1,0:T(8,128)(2,1)}), bf16[16,6,2048]{2,1,0:T(8,128)(2,1)S(1)}, u32[]{:S(2)}, u32[]{:S(2)}) async-start(bf16[16,6,2048]{2,1,0:T(8,128)(2,1)} %reshape.165), calls=%async_computation | async-start | bytes 1048576 | tf_op jit(solution)/shard_map/all_to_all | solution.py:82
  64.1 33.4 %reduce-scatter.2.cloned.1.call-start = ((), (), s32[]{:S(2)}) async-start(), calls=%async_computation.4 | async-start | bytes 589824 | tf_op jit(solution)/shard_map/reduce_scatter | solution.py:90
  88.3 18.0 %copy-start.5 = (f32[24,2]{0,1:T(2,128)S(1)}, f32[24,2]{0,1:T(2,128)}, u32[]{:S(2)}) copy-start(f32[24,2]{0,1:T(2,128)} %param.30) | copy-start | bytes 580
  99.2 17.1 %all-to-all-start.1 = ((bf16[16,6,1024]{2,1,0:T(8,128)(2,1)}), bf16[16,6,1024]{2,1,0:T(8,128)(2,1)S(1)}, u32[]{:S(2)}, u32[]{:S(2)}) async-start(bf16[16,6,1024]{2,1,0:T(8,128)(2,1)} %reshape.167), calls=%async_computation.2 | async-start | bytes 524288 | tf_op jit(solution)/shard_map/all_to_all | solution.py:94
  106.3 14.9 %dynamic-slice-start = ((f32[2048]{0:T(1024)}, s32[]{:T(128)}), f32[1024]{0:T(1024)S(1)}, s32[]{:S(2)}) async-start(f32[2048]{0:T(1024)} %param.31, s32[]{:T(128)} %select_n.28), calls=%async_computation.5 | async-start | bytes 8704 | tf_op jit(solution)/shard_map/dynamic_slice | solution.py:107
Sparse Core Ops, SparseCore 0:
  32.3 20.5 all-reduce.1
  88.4 9.0 reduce-scatter.1
where the time goes:
time: 130 us; the launch traced here: 129 us
  waiting for transfers between devices  33 us (25%)
  local copies, waits for them, and re-layouts  27.5 us (21%)
  matrix products  22 us (17%)
  other arithmetic  16.2 us (12%)
  between operations  14.3 us (11%)
  starting transfers between devices  13.6 us (10%)
  blocking collectives  2.17 us (2%)
    psum x1, waiting for transfers between devices, per_device(): mixed = lax.psum(own_part.astype(jnp.bfloat16), 'tp').astype(jnp.float32)  19.9 us
    all_to_all x1, waiting for transfers between devices, per_device(): lax.all_to_all(results, 'ep', split_axis=0, concat_axis=0, tiled=True)  9.99 us
    mul x2, local copies, waits for them, and re-layouts, per_device(): forget[..., None] * previous  9.72 us
    dot_general x1, matrix products, per_device(): jnp.einsum('shi,shij->shj', act_query, new_state, precision=lax.Precision...  9.61 us
    all_to_all x1, starting transfers between devices, per_device(): lax.all_to_all(outgoing, 'ep', split_axis=0, concat_axis=0, tiled=True)  6.82 us
    all_to_all x1, starting transfers between devices, per_device(): lax.all_to_all(results, 'ep', split_axis=0, concat_axis=0, tiled=True)  6.74 us
    add x1, other arithmetic, per_device(): forget[..., None] * previous  6.17 us
    reshape x1, local copies, waits for them, and re-layouts, per_device(): previous = old_state.reshape(row_count, heads_here, head_dim, head_dim)  6.14 us
  transfers between devices with their start and end apart: 4, of which 3 were waited for; matrix products, arithmetic and copies ran while one was open for 21% of the time, Pallas kernels for 0%

commit v1 on v0

v1 whole, which is shorter than its diff:
```python
import functools

import jax
import jax.numpy as jnp
from jax import lax
from jax.experimental import pallas as pl
from jax.experimental.pallas import tpu as pltpu
from jax.sharding import PartitionSpec as P

F32 = jnp.float32
BF16 = jnp.bfloat16
MESH = pl.DeviceIdType.MESH


def silu(values):
    return values * jax.nn.sigmoid(values)


def mixer_kernel(
    tok, lb, hg, st_hbm, wq_hbm, wf_hbm, wv_hbm, wg_hbm, wo_hbm,
    ns_hbm, part,
    wq, wf, wv, wg, wo, st, ns, spread, qs, fs, vs, ro, mix, sems, out_sems,
):
    rows, heads, width = st.shape
    hd = hg.shape[1]
    loads = [
        pltpu.make_async_copy(src, dst, sems.at[at])
        for at, (src, dst) in enumerate(
            ((wf_hbm, wf), (wv_hbm, wv), (wq_hbm, wq), (st_hbm, st), (wg_hbm, wg), (wo_hbm, wo))
        )
    ]
    for load in loads:
        load.start()
    key_of = lax.broadcasted_iota(jnp.int32, spread.shape, 0) % hd
    lane_key = lax.broadcasted_iota(jnp.int32, spread.shape, 1) // hd
    spread[...] = jnp.where(key_of == lane_key, 1.0, 0.0).astype(BF16)

    def split_heads(values, ref):
        high = values.astype(BF16).astype(F32)
        low = values - high
        for h in range(heads):
            at = slice(h * hd, (h + 1) * hd)
            ref[:, h, 0:hd] = high[:, at]
            ref[:, h, hd : 2 * hd] = low[:, at]

    tokens = tok[...]
    loads[0].wait()
    f_lin = jnp.dot(tokens, wf[...], preferred_element_type=F32)
    bound = lb[...]
    split_heads(bound + (1.0 - bound) * jax.nn.sigmoid(f_lin), fs)
    loads[1].wait()
    v_lin = jnp.dot(tokens, wv[...], preferred_element_type=F32)
    for h in range(heads):
        at = slice(h * hd, (h + 1) * hd)
        vs[:, h, 0:hd] = v_lin[:, at]
        vs[:, h, hd : 2 * hd] = v_lin[:, at]
    loads[2].wait()
    q_lin = jnp.dot(tokens, wq[...], preferred_element_type=F32)
    split_heads(silu(q_lin), qs)
    loads[3].wait()
    flat = (rows * heads, 2 * hd)
    keep = fs[...].reshape(flat).astype(BF16)
    ask = qs[...].reshape(flat).astype(BF16)
    value = vs[...]
    pair = 2 * hd
    block = 2 * pair
    chunks = out_sems.shape[0]
    per_chunk = width // chunks
    acc = jnp.zeros((rows, heads, pair), F32)
    stores = []
    for chunk in range(chunks):

        def step(i, acc, chunk=chunk):
            start = pl.multiple_of(chunk * per_chunk + i * block, block)
            ones = spread[:, pl.ds(start, block)]
            f_wide = jnp.dot(keep, ones, preferred_element_type=F32).reshape(rows, heads, block)
            q_wide = jnp.dot(ask, ones, preferred_element_type=F32).reshape(rows, heads, block)
            for half in range(2):
                lanes = pl.ds(pl.multiple_of(start + half * pair, pair), pair)
                cut = slice(half * pair, (half + 1) * pair)
                new = value + f_wide[:, :, cut] * (st[:, :, lanes] - value)
                ns[:, :, lanes] = new
                acc = acc + q_wide[:, :, cut] * new
            return acc

        acc = lax.fori_loop(0, per_chunk // block, step, acc)
        span = pl.ds(chunk * per_chunk, per_chunk)
        store = pltpu.make_async_copy(ns.at[:, :, span], ns_hbm.at[:, :, span], out_sems.at[chunk])
        store.start()
        stores.append(store)
    readout = acc[:, :, 0:hd] + acc[:, :, hd:pair]
    square = jnp.mean(readout * readout, -1, keepdims=True)
    ro[...] = readout * lax.rsqrt(square + 1e-06) * hg[...].reshape(1, 1, hd)
    for h in range(heads):
        mix[:, h * hd : (h + 1) * hd] = ro[:, h, :]
    loads[4].wait()
    g_lin = jnp.dot(tokens, wg[...], preferred_element_type=F32)
    mixer_out = (mix[...] * silu(g_lin)).astype(BF16)
    loads[5].wait()
    part[...] = jnp.dot(mixer_out, wo[...], preferred_element_type=F32).astype(BF16)
    for store in stores:
        store.wait()


def expert_kernel(
    capacity, n,
    part, tok, mix_gain, ids, route, moe_gain, eg_hbm, eu_hbm, ed_hbm,
    out,
    eg, eu, ed, part_in, am, outgoing, mine, theirs, down_out, down_in, results, back,
    stat_out, stat_in,
    w_sems, pair_sems, s1, r1, s2, r2, fs, fr, ds_, dr,
):
    e = lax.axis_index("ep")
    c = lax.axis_index("tp")
    other = 1 - c
    rows, width = tok.shape
    slots = outgoing.shape[1]
    half = width // 2
    total = n * slots
    barrier = pltpu.get_barrier_semaphore()
    pl.semaphore_signal(barrier, inc=1, device_id=(e, other), device_id_type=MESH)
    for d in range(1, n):
        pl.semaphore_signal(barrier, inc=1, device_id=(lax.rem(e + d, n), c), device_id_type=MESH)
    loads = [
        pltpu.make_async_copy(src, dst, w_sems.at[at])
        for at, (src, dst) in enumerate(((eg_hbm, eg), (eu_hbm, eu), (ed_hbm, ed)))
    ]
    for load in loads:
        load.start()

    def remote(src, dst, send, recv, device):
        return pltpu.make_async_remote_copy(
            src_ref=src, dst_ref=dst, send_sem=send, recv_sem=recv,
            device_id=device, device_id_type=MESH,
        )

    lane = lax.broadcasted_iota(jnp.int32, (rows, total), 1)
    lane_expert = lane // slots
    lane_rank = (lane % slots).astype(F32)
    first = jnp.where(ids[:, 0:1] == lane_expert, 1.0, 0.0)
    second = jnp.where(ids[:, 1:2] == lane_expert, 1.0, 0.0)
    named = first + second
    row_at = lax.broadcasted_iota(jnp.int32, (rows, rows), 0)
    col_at = lax.broadcasted_iota(jnp.int32, (rows, rows), 1)
    earlier = jnp.where(col_at < row_at, 1.0, 0.0).astype(BF16)
    before = jnp.dot(earlier, named.astype(BF16), preferred_element_type=F32)
    place = jnp.where(before == lane_rank, named, 0.0)
    weigh = place * (first * route[:, 0:1] + second * route[:, 1:2])
    weigh_high = weigh.astype(BF16)
    weigh_low = (weigh - weigh_high.astype(F32)).astype(BF16)
    place_t = jnp.transpose(place).astype(BF16)

    pl.semaphore_wait(barrier, n)
    swap = remote(part, part_in, pair_sems.at[0], pair_sems.at[1], (e, other))
    swap.start()
    base = tok[...].astype(F32) + part[...].astype(F32)
    swap.wait()
    values = base + part_in[...].astype(F32)
    centered = values - jnp.mean(values, -1, keepdims=True)
    variance = jnp.mean(centered * centered, -1, keepdims=True)
    am[...] = centered * lax.rsqrt(variance + 1e-05) * mix_gain[...]

    own_cols = pl.ds(pl.multiple_of(c * half, half), half)
    other_cols = pl.ds(pl.multiple_of(other * half, half), half)
    am_half = am[:, own_cols].astype(BF16)
    sent = jnp.dot(place_t, am_half, preferred_element_type=F32)
    for at in range(n):
        outgoing[at] = sent[at * slots : (at + 1) * slots].astype(BF16)
    sends = []
    for d in range(1, n):
        peer = lax.rem(e + d, n)
        copy = remote(outgoing.at[peer], mine.at[e], s1.at[d], r1.at[d], (peer, c))
        copy.start()
        sends.append(copy)
    forwards = [remote(outgoing.at[e], theirs.at[e], fs.at[0], fr.at[0], (e, other))]
    forwards[0].start()
    mine[pl.ds(e, 1)] = outgoing[pl.ds(e, 1)]
    for d in range(1, n):
        sends[d - 1].wait_recv()
        source = lax.rem(e - d + n, n)
        copy = remote(mine.at[source], theirs.at[source], fs.at[d], fr.at[d], (e, other))
        copy.start()
        forwards.append(copy)

    def flat(ref):
        return ref[...].astype(F32).reshape(total, half).astype(BF16)

    for load in loads:
        load.wait()
    own_rows = flat(mine)
    gate = jnp.dot(own_rows, eg[own_cols, :], preferred_element_type=F32)
    up = jnp.dot(own_rows, eu[own_cols, :], preferred_element_type=F32)
    for copy in forwards:
        copy.wait_recv()
    other_rows = flat(theirs)
    gate = gate + jnp.dot(other_rows, eg[other_cols, :], preferred_element_type=F32)
    up = up + jnp.dot(other_rows, eu[other_cols, :], preferred_element_type=F32)
    hidden = (silu(gate) * up).astype(BF16)

    pieces = ds_.shape[0]
    span = n // pieces
    height = span * slots
    downs = []
    for piece in range(pieces):
        block = jnp.dot(
            hidden[piece * height : (piece + 1) * height], ed[:, other_cols],
            preferred_element_type=F32,
        )
        for at in range(span):
            down_out[piece * span + at] = block[at * slots : (at + 1) * slots].astype(BF16)
        here = pl.ds(piece * span, span)
        copy = remote(
            down_out.at[here], down_in.at[here], ds_.at[piece], dr.at[piece], (e, other)
        )
        copy.start()
        downs.append(copy)
    kept = jnp.dot(hidden, ed[:, own_cols], preferred_element_type=F32)
    for piece in range(pieces):
        downs[piece].wait_recv()
        for at in range(piece * span, (piece + 1) * span):
            own = kept[at * slots : (at + 1) * slots].astype(BF16).astype(F32)
            results[at] = (own + down_in[at].astype(F32)).astype(BF16)
    returns = []
    for d in range(1, n):
        peer = lax.rem(e + d, n)
        copy = remote(results.at[peer], back.at[e], s2.at[d], r2.at[d], (peer, c))
        copy.start()
        returns.append(copy)
    back[pl.ds(e, 1)] = results[pl.ds(e, 1)]
    for copy in returns:
        copy.wait_recv()
    picked = flat(back)
    moe_sum = jnp.dot(weigh_high, picked, preferred_element_type=F32) + jnp.dot(
        weigh_low, picked, preferred_element_type=F32
    )
    final = am_half.astype(F32) + moe_sum
    mean_own = jnp.mean(final, -1, keepdims=True)
    off = final - mean_own
    spread_own = jnp.sum(off * off, -1, keepdims=True)
    stat_lane = lax.broadcasted_iota(jnp.int32, stat_out.shape, 1)
    stat_out[...] = jnp.where(stat_lane < stat_out.shape[1] // 2, mean_own, spread_own)
    stats = remote(stat_out, stat_in, pair_sems.at[2], pair_sems.at[3], (e, other))
    stats.start()
    for copy in sends + forwards + downs + returns:
        copy.wait_send()
    stats.wait()
    mean_other = stat_in[:, 0:1]
    last = stat_in.shape[1]
    spread_other = stat_in[:, last - 1 : last]
    gap = mean_other - mean_own
    variance = (spread_own + spread_other + gap * gap * (half / 2)) / width
    gain = moe_gain[:, own_cols]
    out[...] = ((off - 0.5 * gap) * lax.rsqrt(variance + 1e-05) * gain).astype(BF16)


def per_device(
    tokens, old_state, w_query, w_forget, w_value, w_gate, lower_bound, head_gain, w_out,
    mix_gain, expert_gate, expert_up, expert_down, expert_ids, route_weight, moe_gain,
):
    rows, width = tokens.shape
    heads, state_width = old_state.shape[1:]
    hd = head_gain.shape[0]
    cols = w_query.shape[1]
    n = lax.axis_size("ep")
    half = width // lax.axis_size("tp")
    top = expert_ids.shape[1]
    capacity = max(2, 2 * top * rows // n)
    slots = -(-capacity // 8) * 8
    vmem = pl.BlockSpec(memory_space=pltpu.VMEM)
    hbm = pl.BlockSpec(memory_space=pl.ANY)
    new_state, part = pl.pallas_call(
        mixer_kernel,
        out_shape=(
            jax.ShapeDtypeStruct(old_state.shape, F32),
            jax.ShapeDtypeStruct((rows, width), BF16),
        ),
        in_specs=[vmem] * 3 + [hbm] * 6,
        out_specs=(hbm, vmem),
        scratch_shapes=[
            pltpu.VMEM((width, cols), BF16),
            pltpu.VMEM((width, cols), BF16),
            pltpu.VMEM((width, cols), BF16),
            pltpu.VMEM((width, cols), BF16),
            pltpu.VMEM((cols, width), BF16),
            pltpu.VMEM(old_state.shape, F32),
            pltpu.VMEM(old_state.shape, F32),
            pltpu.VMEM((2 * hd, state_width), BF16),
            pltpu.VMEM((rows, heads, 2 * hd), F32),
            pltpu.VMEM((rows, heads, 2 * hd), F32),
            pltpu.VMEM((rows, heads, 2 * hd), F32),
            pltpu.VMEM((rows, heads, hd), F32),
            pltpu.VMEM((rows, cols), F32),
            pltpu.SemaphoreType.DMA((6,)),
            pltpu.SemaphoreType.DMA((4,)),
        ],
        compiler_params=pltpu.CompilerParams(vmem_limit_bytes=48 * 1024 * 1024),
        name="mixer",
    )(
        tokens, lower_bound.reshape(1, cols), head_gain.reshape(1, hd),
        old_state, w_query, w_forget, w_value, w_gate, w_out,
    )
    ff = expert_gate.shape[2]
    slab = pltpu.VMEM((n, slots, half), BF16)
    pieces = 4
    dma = pltpu.SemaphoreType.DMA
    next_tokens = pl.pallas_call(
        functools.partial(expert_kernel, capacity, n),
        out_shape=jax.ShapeDtypeStruct((rows, half), BF16),
        in_specs=[vmem] * 6 + [hbm] * 3,
        out_specs=vmem,
        scratch_shapes=[
            pltpu.VMEM((width, ff), BF16),
            pltpu.VMEM((width, ff), BF16),
            pltpu.VMEM((ff, width), BF16),
            pltpu.VMEM((rows, width), BF16),
            pltpu.VMEM((rows, width), F32),
            slab, slab, slab, slab, slab, slab, slab,
            pltpu.VMEM((rows, 128), F32),
            pltpu.VMEM((rows, 128), F32),
            dma((3,)), dma((4,)), dma((n,)), dma((n,)), dma((n,)), dma((n,)), dma((n,)), dma((n,)),
            dma((pieces,)), dma((pieces,)),
        ],
        compiler_params=pltpu.CompilerParams(
            collective_id=0, has_side_effects=True, vmem_limit_bytes=48 * 1024 * 1024
        ),
        name="experts",
    )(
        part, tokens, mix_gain.reshape(1, width), expert_ids, route_weight,
        moe_gain.reshape(1, width), expert_gate.reshape(width, ff), expert_up.reshape(width, ff),
        expert_down.reshape(ff, width),
    )
    return (next_tokens, new_state)


def solution(mesh):
    in_specs = (
        P("ep", None),
        P("ep", "tp", None),
        P(None, "tp"),
        P(None, "tp"),
        P(None, "tp"),
        P(None, "tp"),
        P("tp"),
        P(),
        P("tp", None),
        P(),
        P("ep", None, "tp"),
        P("ep", None, "tp"),
        P("ep", "tp", None),
        P("ep", None),
        P("ep", None),
        P(),
    )
    out_specs = (P("ep", "tp"), P("ep", "tp", None))
    return jax.shard_map(
        per_device, mesh=mesh, in_specs=in_specs, out_specs=out_specs, check_vma=False
    )
```

time: 130 us -> 44 us (0.34)
  Pallas kernels: 0 us -> 35.5 us
  waiting for transfers between devices: 33 us -> 0 us
  matrix products: 22 us -> 0 us
  local copies, waits for them, and re-layouts: 27.5 us -> 7.57 us
  other arithmetic: 16.2 us -> 0 us
  between operations: 14.3 us -> 0.7 us
  starting transfers between devices: 13.6 us -> 0 us
  blocking collectives: 2.17 us -> 0 us
    pallas_call x0 -> x2, Pallas kernels: none -> 35.5 us  [the longest x1 27.5 us: per_device(): pl.pallas_call(functools.partial(expert_kernel, capacity, n), out_shape=j...]
    dot_general x9 -> x0, matrix products: 22 us -> none  [the longest x1 9.61 us: per_device(): jnp.einsum('shi,shij->shj', act_query, new_state, precision=lax.Precision...]
    psum x1 -> x0, waiting for transfers between devices: 19.9 us -> none  [per_device(): mixed = lax.psum(own_part.astype(jnp.bfloat16), 'tp').astype(jnp.float32)]
    mul x6 -> x0, local copies, waits for them, and re-layouts: 15.8 us -> none  [the longest x2 9.72 us: per_device(): forget[..., None] * previous]
    all_to_all x2 -> x0, starting transfers between devices: 13.6 us -> none  [the longest x1 6.82 us: per_device(): lax.all_to_all(outgoing, 'ep', split_axis=0, concat_axis=0, tiled=True)]
    all_to_all x2 -> x0, waiting for transfers between devices: 9.99 us -> none  [the longest x1 9.99 us: per_device(): lax.all_to_all(results, 'ep', split_axis=0, concat_axis=0, tiled=True)]
    reshape x8 -> x0, local copies, waits for them, and re-layouts: 9.29 us -> none  [the longest x1 6.14 us: per_device(): previous = old_state.reshape(row_count, heads_here, head_dim, head_dim)]
    unnamed x16 -> x23, local copies, waits for them, and re-layouts: 0.22 us -> 7.57 us
  transfers between devices with their start and end apart: 4 -> 0, of which waited for: 3 -> 0; matrix products, arithmetic and copies ran while one was open for 21% -> 0% of each run, Pallas kernels for 0% -> 0%
where the time goes in v1:
time: 44 us; the launch traced here: 43.7 us
  Pallas kernels  35.5 us (81%)
  local copies, waits for them, and re-layouts  7.57 us (17%)
  between operations  0.7 us (2%)
    pallas_call x1, Pallas kernels, per_device(): pl.pallas_call(functools.partial(expert_kernel, capacity, n), out_shape=j...  27.5 us
    pallas_call x1, Pallas kernels, per_device(): pl.pallas_call(mixer_kernel, out_shape=(jax.ShapeDtypeStruct(old_state.sh...  7.99 us
    unnamed x23, local copies, waits for them, and re-layouts  7.57 us

profile of v1, /device:TPU:0, one launch (start us, length us, event | category | flops | bytes accessed | tf_op | source)
XLA Modules:
  0.0 43.7 jit_solution(11469444607216836099)
XLA Ops:
  0.6 0.8 %copy.18.ids = s32[24,2]{1,0:T(8,128)S(1)} copy(s32[24,2]{0,1:T(2,128)} %param.29) | data formatting | bytes 384 | tf_op args[13]
  1.4 0.8 %copy.19.route = f32[24,2]{1,0:T(8,128)S(1)} copy(f32[24,2]{0,1:T(2,128)} %param.30) | data formatting | bytes 384 | tf_op args[14]
  2.1 0.0 copy-start
  2.1 1.6 %copy-done = bf16[2048,512]{1,0:T(8,128)(2,1)S(1)} copy-done((bf16[2048,512]{1,0:T(8,128)(2,1)S(1)}, bf16[2048,512]{1,0:T(8,128)(2,1)}, u32[]{:S(2)}) %copy-start) | copy-done | bytes 2097176
  3.7 0.0 copy-start.1
  3.7 1.6 %copy-done.1 = bf16[2048,512]{1,0:T(8,128)(2,1)S(1)} copy-done((bf16[2048,512]{1,0:T(8,128)(2,1)S(1)}, bf16[2048,512]{1,0:T(8,128)(2,1)}, u32[]{:S(2)}) %copy-start.1) | copy-done | bytes 2097176
  5.3 0.0 copy-start.5
  5.3 0.9 %copy-done.5 = bf16[24,2048]{1,0:T(8,128)(2,1)S(1)} copy-done((bf16[24,2048]{1,0:T(8,128)(2,1)S(1)}, bf16[24,2048]{1,0:T(8,128)(2,1)}, u32[]{:S(2)}) %copy-start.5) | copy-done | bytes 98328
  6.2 0.0 copy-start.8
  6.2 0.7 %copy-done.8 = f32[512]{0:T(512)S(1)} copy-done((f32[512]{0:T(512)S(1)}, f32[512]{0:T(512)}, u32[]{:S(2)}) %copy-start.8) | copy-done | bytes 2072
  6.9 0.0 copy-start.9
  6.9 0.7 %copy-done.9 = f32[64]{0:T(128)S(1)} copy-done((f32[64]{0:T(128)S(1)}, f32[64]{0:T(128)}, u32[]{:S(2)}) %copy-start.9) | copy-done | bytes 280
  7.6 0.0 copy-start.2
  7.6 0.0 copy-start.3
  7.6 0.0 copy-start.4
  7.6 0.0 copy-start.6
  7.6 0.0 copy-start.7
  7.6 8.0 %mixer.1 = (f32[24,8,4096]{2,1,0:T(8,128)}, bf16[24,2048]{1,0:T(8,128)(2,1)S(1)}) custom-call(bf16[24,2048]{1,0:T(8,128)(2,1)S(1)} %copy-done.5, f32[1,512]{1,0:T(1,128)S(1)} %bitcast.12, f32[1,64]{1,0:T(1,128)S(1)} %bitcast.13, f32[24,8,4096]{2,1,0:T(8,128)} %st_hbm.1, bf16[2048,512]{1,0:T(8,128)(2,1)S(1)} %copy-done, bf16[2048,512]{1,0:T(8,128)(2,1)S(1)} %copy-done.1, ...), custom_call_target="tpu_custom_call" | custom-call | tf_op jit(solution)/shard_map/mixer/pallas_call | solution.py:271
  15.6 0.0 copy-done.2
  15.6 0.0 copy-done.3
  15.6 0.0 copy-done.4
  15.6 0.0 copy-done.6
  15.6 0.0 copy-done.7
  15.6 27.5 %experts.1 = bf16[24,1024]{1,0:T(8,128)(2,1)S(1)} custom-call(bf16[24,2048]{1,0:T(8,128)(2,1)S(1)} %get-tuple-element.4.part, bf16[24,2048]{1,0:T(8,128)(2,1)S(1)} %copy-done.5, f32[1,2048]{1,0:T(1,128)S(1)} %bitcast.10, s32[24,2]{1,0:T(8,128)S(1)} %copy.18.ids, f32[24,2]{1,0:T(8,128)S(1)} %copy.19.route, f32[1,2048]{1,0:T(1,128)S(1)} %bitcast.11, ...), custom_call_target="tpu_custom_call" | custom-call | tf_op jit(solution)/shard_map/experts/pallas_call | solution.py:306
  43.1 0.6 %copy.21 = bf16[24,1024]{1,0:T(8,128)(2,1)} copy(bf16[24,1024]{1,0:T(8,128)(2,1)S(1)} %experts.1) | data formatting | bytes 98304
Async XLA Ops:
  2.1 1.6 %copy-start = (bf16[2048,512]{1,0:T(8,128)(2,1)S(1)}, bf16[2048,512]{1,0:T(8,128)(2,1)}, u32[]{:S(2)}) copy-start(bf16[2048,512]{1,0:T(8,128)(2,1)} %wq_hbm.1) | copy-start | bytes 6291460
  3.7 1.6 %copy-start.1 = (bf16[2048,512]{1,0:T(8,128)(2,1)S(1)}, bf16[2048,512]{1,0:T(8,128)(2,1)}, u32[]{:S(2)}) copy-start(bf16[2048,512]{1,0:T(8,128)(2,1)} %wf_hbm.1) | copy-start | bytes 6291460
  5.3 0.9 %copy-start.5 = (bf16[24,2048]{1,0:T(8,128)(2,1)S(1)}, bf16[24,2048]{1,0:T(8,128)(2,1)}, u32[]{:S(2)}) copy-start(bf16[24,2048]{1,0:T(8,128)(2,1)} %tok.3) | copy-start | bytes 294916
  6.2 0.7 %copy-start.8 = (f32[512]{0:T(512)S(1)}, f32[512]{0:T(512)}, u32[]{:S(2)}) copy-start(f32[512]{0:T(512)} %param.22) | copy-start | bytes 6148
  6.9 0.7 %copy-start.9 = (f32[64]{0:T(128)S(1)}, f32[64]{0:T(128)}, u32[]{:S(2)}) copy-start(f32[64]{0:T(128)} %param.23) | copy-start | bytes 772
  7.6 8.0 %copy-start.2 = (bf16[1,2048,256]{2,1,0:T(8,128)(2,1)S(1)}, bf16[1,2048,256]{2,1,0:T(8,128)(2,1)}, u32[]{:S(2)}) copy-start(bf16[1,2048,256]{2,1,0:T(8,128)(2,1)} %param.26) | copy-start | bytes 3145732
  7.6 8.0 %copy-start.3 = (bf16[1,2048,256]{2,1,0:T(8,128)(2,1)S(1)}, bf16[1,2048,256]{2,1,0:T(8,128)(2,1)}, u32[]{:S(2)}) copy-start(bf16[1,2048,256]{2,1,0:T(8,128)(2,1)} %param.27) | copy-start | bytes 3145732
  7.6 8.0 %copy-start.4 = (bf16[1,256,2048]{2,1,0:T(8,128)(2,1)S(1)}, bf16[1,256,2048]{2,1,0:T(8,128)(2,1)}, u32[]{:S(2)}) copy-start(bf16[1,256,2048]{2,1,0:T(8,128)(2,1)} %param.28) | copy-start | bytes 3145732
  7.6 8.1 %copy-start.6 = (f32[2048]{0:T(1024)S(1)}, f32[2048]{0:T(1024)}, u32[]{:S(2)}) copy-start(f32[2048]{0:T(1024)} %param.25) | copy-start | bytes 24580
  7.6 8.1 %copy-start.7 = (f32[2048]{0:T(1024)S(1)}, f32[2048]{0:T(1024)}, u32[]{:S(2)}) copy-start(f32[2048]{0:T(1024)} %param.31) | copy-start | bytes 24580

commit v2 on v1

--- a/solution.py
+++ b/solution.py
@@ -10,6 +10,7 @@
 F32 = jnp.float32
 BF16 = jnp.bfloat16
 MESH = pl.DeviceIdType.MESH
+GRANT = 67043328 - 512 * 1024
 
 
 def silu(values):
@@ -17,9 +18,9 @@
 
 
 def mixer_kernel(
-    tok, lb, hg, st_hbm, wq_hbm, wf_hbm, wv_hbm, wg_hbm, wo_hbm,
+    tok_hbm, lb_hbm, hg_hbm, st_hbm, wq_hbm, wf_hbm, wv_hbm, wg_hbm, wo_hbm,
     ns_hbm, part,
-    wq, wf, wv, wg, wo, st, ns, spread, qs, fs, vs, ro, mix, sems, out_sems,
+    tok, lb, hg, wq, wf, wv, wg, wo, st, ns, spread, qs, fs, vs, ro, mix, sems, out_sems,
 ):
     rows, heads, width = st.shape
     hd = hg.shape[1]
@@ -29,7 +30,11 @@
             ((wf_hbm, wf), (wv_hbm, wv), (wq_hbm, wq), (st_hbm, st), (wg_hbm, wg), (wo_hbm, wo))
         )
     ]
-    for load in loads:
+    smalls = [
+        pltpu.make_async_copy(src, dst, sems.at[len(loads) + at])
+        for at, (src, dst) in enumerate(((tok_hbm, tok), (lb_hbm, lb), (hg_hbm, hg)))
+    ]
+    for load in smalls + loads:
         load.start()
     key_of = lax.broadcasted_iota(jnp.int32, spread.shape, 0) % hd
     lane_key = lax.broadcasted_iota(jnp.int32, spread.shape, 1) // hd
@@ -43,6 +48,8 @@
             ref[:, h, 0:hd] = high[:, at]
             ref[:, h, hd : 2 * hd] = low[:, at]
 
+    for load in smalls:
+        load.wait()
     tokens = tok[...]
     loads[0].wait()
     f_lin = jnp.dot(tokens, wf[...], preferred_element_type=F32)
@@ -104,8 +111,9 @@
 
 def expert_kernel(
     capacity, n,
-    part, tok, mix_gain, ids, route, moe_gain, eg_hbm, eu_hbm, ed_hbm,
+    part_hbm, tok_hbm, mix_hbm, ids_hbm, route_hbm, moe_hbm, eg_hbm, eu_hbm, ed_hbm,
     out,
+    part, tok, mix_gain, ids, route, moe_gain,
     eg, eu, ed, part_in, am, outgoing, mine, theirs, down_out, down_in, results, back,
     stat_out, stat_in,
     w_sems, pair_sems, s1, r1, s2, r2, fs, fr, ds_, dr,
@@ -114,8 +122,10 @@
     c = lax.axis_index("tp")
     other = 1 - c
     rows, width = tok.shape
-    slots = outgoing.shape[1]
+    slots, wide = outgoing.shape[1:]
     half = width // 2
+    quarter = half - wide
+    folds = wide // quarter if quarter else 0
     total = n * slots
     barrier = pltpu.get_barrier_semaphore()
     pl.semaphore_signal(barrier, inc=1, device_id=(e, other), device_id_type=MESH)
@@ -123,7 +133,13 @@
         pl.semaphore_signal(barrier, inc=1, device_id=(lax.rem(e + d, n), c), device_id_type=MESH)
     loads = [
         pltpu.make_async_copy(src, dst, w_sems.at[at])
-        for at, (src, dst) in enumerate(((eg_hbm, eg), (eu_hbm, eu), (ed_hbm, ed)))
+        for at, (src, dst) in enumerate(
+            (
+                (ids_hbm, ids), (route_hbm, route), (part_hbm, part), (tok_hbm, tok),
+                (mix_hbm, mix_gain), (moe_hbm, moe_gain),
+                (eg_hbm, eg), (eu_hbm, eu), (ed_hbm, ed),
+            )
+        )
     ]
     for load in loads:
         load.start()
@@ -134,24 +150,46 @@
             device_id=device, device_id_type=MESH,
         )
 
-    lane = lax.broadcasted_iota(jnp.int32, (rows, total), 1)
-    lane_expert = lane // slots
-    lane_rank = (lane % slots).astype(F32)
-    first = jnp.where(ids[:, 0:1] == lane_expert, 1.0, 0.0)
-    second = jnp.where(ids[:, 1:2] == lane_expert, 1.0, 0.0)
+    for load in loads[:6]:
+        load.wait()
+    slot = lax.broadcasted_iota(jnp.int32, (total, rows), 0)
+    slot_expert = slot // slots
+    slot_rank = slot % slots
+    first = jnp.where(ids[0:1, :] == slot_expert, 1.0, 0.0)
+    second = jnp.where(ids[1:2, :] == slot_expert, 1.0, 0.0)
     named = first + second
     row_at = lax.broadcasted_iota(jnp.int32, (rows, rows), 0)
     col_at = lax.broadcasted_iota(jnp.int32, (rows, rows), 1)
-    earlier = jnp.where(col_at < row_at, 1.0, 0.0).astype(BF16)
-    before = jnp.dot(earlier, named.astype(BF16), preferred_element_type=F32)
-    place = jnp.where(before == lane_rank, named, 0.0)
-    weigh = place * (first * route[:, 0:1] + second * route[:, 1:2])
-    weigh_high = weigh.astype(BF16)
-    weigh_low = (weigh - weigh_high.astype(F32)).astype(BF16)
-    place_t = jnp.transpose(place).astype(BF16)
+    earlier = jnp.where(row_at < col_at, 1.0, 0.0).astype(BF16)
+    before = jnp.dot(named.astype(BF16), earlier, preferred_element_type=F32)
+    places = [jnp.where(before == slot_rank.astype(F32), named, 0.0)]
+    for p in range(folds):
+        rank = (slot_rank - capacity) * folds + p
+        hit = (before == rank.astype(F32)) & (slot_rank >= capacity)
+        places.append(jnp.where(hit, named, 0.0))
+    route_of = first * route[0:1, :] + second * route[1:2, :]
+    weighs = []
+    for place in places:
+        weigh = jnp.transpose(place * route_of)
+        high = weigh.astype(BF16).astype(F32)
+        weighs.append(jnp.concatenate([high, weigh - high], 0).astype(BF16))
+    places = [place.astype(BF16) for place in places]
+    to_at = lax.broadcasted_iota(jnp.int32, (total, total), 0)
+    from_at = lax.broadcasted_iota(jnp.int32, (total, total), 1)
+    together = to_at // slots == from_at // slots
+    unfold, refold = [], []
+    for p in range(folds):
+        to_rank, from_rank = to_at % slots, from_at % slots
+        un = together & (from_rank >= capacity) & (to_rank == (from_rank - capacity) * folds + p)
+        re = together & (to_rank >= capacity) & (from_rank == (to_rank - capacity) * folds + p)
+        unfold.append(jnp.where(un, 1.0, 0.0).astype(BF16))
+        refold.append(jnp.where(re, 1.0, 0.0).astype(BF16))
+
+    def cut(values, p):
+        return values[:, p * quarter : (p + 1) * quarter]
 
     pl.semaphore_wait(barrier, n)
-    swap = remote(part, part_in, pair_sems.at[0], pair_sems.at[1], (e, other))
+    swap = remote(part_hbm, part_in, pair_sems.at[0], pair_sems.at[1], (e, other))
     swap.start()
     base = tok[...].astype(F32) + part[...].astype(F32)
     swap.wait()
@@ -163,7 +201,12 @@
     own_cols = pl.ds(pl.multiple_of(c * half, half), half)
     other_cols = pl.ds(pl.multiple_of(other * half, half), half)
     am_half = am[:, own_cols].astype(BF16)
-    sent = jnp.dot(place_t, am_half, preferred_element_type=F32)
+    sent = jnp.dot(places[0], am_half[:, 0:wide], preferred_element_type=F32)
+    if folds:
+        tail = am_half[:, wide:half]
+        sent = sent + jnp.concatenate(
+            [jnp.dot(place, tail, preferred_element_type=F32) for place in places[1:]], 1
+        )
     for at in range(n):
         outgoing[at] = sent[at * slots : (at + 1) * slots].astype(BF16)
     sends = []
@@ -183,29 +226,57 @@
         forwards.append(copy)
 
     def flat(ref):
-        return ref[...].astype(F32).reshape(total, half).astype(BF16)
-
-    for load in loads:
+        return ref[...].astype(F32).reshape(total, wide).astype(BF16)
+
+    def gate_and_up(ref, side):
+        block = flat(ref)
+        start = pl.multiple_of(side * half, half)
+        cols = pl.ds(start, wide)
+        gate = jnp.dot(block, eg[cols, :], preferred_element_type=F32)
+        up = jnp.dot(block, eu[cols, :], preferred_element_type=F32)
+        if folds:
+            tail = jnp.zeros((total, quarter), F32)
+            for p in range(folds):
+                tail = tail + jnp.dot(unfold[p], cut(block, p), preferred_element_type=F32)
+            tail = tail.astype(BF16)
+            cols = pl.ds(pl.multiple_of(start + wide, quarter), quarter)
+            gate = gate + jnp.dot(tail, eg[cols, :], preferred_element_type=F32)
+            up = up + jnp.dot(tail, eu[cols, :], preferred_element_type=F32)
+        return gate, up
+
+    for load in loads[6:]:
         load.wait()
-    own_rows = flat(mine)
-    gate = jnp.dot(own_rows, eg[own_cols, :], preferred_element_type=F32)
-    up = jnp.dot(own_rows, eu[own_cols, :], preferred_element_type=F32)
+    gate, up = gate_and_up(mine, c)
     for copy in forwards:
         copy.wait_recv()
-    other_rows = flat(theirs)
-    gate = gate + jnp.dot(other_rows, eg[other_cols, :], preferred_element_type=F32)
-    up = up + jnp.dot(other_rows, eu[other_cols, :], preferred_element_type=F32)
-    hidden = (silu(gate) * up).astype(BF16)
+    gate_more, up_more = gate_and_up(theirs, other)
+    hidden = silu(gate + gate_more) * (up + up_more)
+    hidden_rank = lax.broadcasted_iota(jnp.int32, hidden.shape, 0) % slots
+    hidden = jnp.where(hidden_rank < capacity, hidden, 0.0).astype(BF16)
 
     pieces = ds_.shape[0]
     span = n // pieces
     height = span * slots
+
+    def down(piece, cols):
+        block = jnp.dot(
+            hidden[piece * height : (piece + 1) * height], ed[:, cols],
+            preferred_element_type=F32,
+        ).astype(BF16)
+        if folds:
+            tail = block[:, wide:half]
+            block = block[:, 0:wide].astype(F32) + jnp.concatenate(
+                [
+                    jnp.dot(one[0:height, 0:height], tail, preferred_element_type=F32)
+                    for one in refold
+                ],
+                1,
+            )
+        return block.astype(F32)
+
     downs = []
     for piece in range(pieces):
-        block = jnp.dot(
-            hidden[piece * height : (piece + 1) * height], ed[:, other_cols],
-            preferred_element_type=F32,
-        )
+        block = down(piece, other_cols)
         for at in range(span):
             down_out[piece * span + at] = block[at * slots : (at + 1) * slots].astype(BF16)
         here = pl.ds(piece * span, span)
@@ -214,12 +285,12 @@
         )
         copy.start()
         downs.append(copy)
-    kept = jnp.dot(hidden, ed[:, own_cols], preferred_element_type=F32)
+    kept = [down(piece, own_cols) for piece in range(pieces)]
     for piece in range(pieces):
         downs[piece].wait_recv()
-        for at in range(piece * span, (piece + 1) * span):
-            own = kept[at * slots : (at + 1) * slots].astype(BF16).astype(F32)
-            results[at] = (own + down_in[at].astype(F32)).astype(BF16)
+        for at in range(span):
+            own = kept[piece][at * slots : (at + 1) * slots]
+            results[piece * span + at] = (own + down_in[piece * span + at].astype(F32)).astype(BF16)
     returns = []
     for d in range(1, n):
         peer = lax.rem(e + d, n)
@@ -230,9 +301,17 @@
     for copy in returns:
         copy.wait_recv()
     picked = flat(back)
-    moe_sum = jnp.dot(weigh_high, picked, preferred_element_type=F32) + jnp.dot(
-        weigh_low, picked, preferred_element_type=F32
-    )
+
+    def weighted(weigh, block):
+        both = jnp.dot(weigh, block, preferred_element_type=F32)
+        return both[0:rows] + both[rows : 2 * rows]
+
+    moe_sum = weighted(weighs[0], picked)
+    if folds:
+        tail = jnp.zeros((rows, quarter), F32)
+        for p in range(folds):
+            tail = tail + weighted(weighs[1 + p], cut(picked, p))
+        moe_sum = jnp.concatenate([moe_sum, tail], 1)
     final = am_half.astype(F32) + moe_sum
     mean_own = jnp.mean(final, -1, keepdims=True)
     off = final - mean_own
@@ -267,16 +346,19 @@
     capacity = max(2, 2 * top * rows // n)
     slots = -(-capacity // 8) * 8
     vmem = pl.BlockSpec(memory_space=pltpu.VMEM)
-    hbm = pl.BlockSpec(memory_space=pl.ANY)
+    hbm = pl.BlockSpec(memory_space=pltpu.MemorySpace.HBM)
     new_state, part = pl.pallas_call(
         mixer_kernel,
         out_shape=(
             jax.ShapeDtypeStruct(old_state.shape, F32),
             jax.ShapeDtypeStruct((rows, width), BF16),
         ),
-        in_specs=[vmem] * 3 + [hbm] * 6,
+        in_specs=[hbm] * 9,
         out_specs=(hbm, vmem),
         scratch_shapes=[
+            pltpu.VMEM((rows, width), BF16),
+            pltpu.VMEM((1, cols), F32),
+            pltpu.VMEM((1, hd), F32),
             pltpu.VMEM((width, cols), BF16),
             pltpu.VMEM((width, cols), BF16),
             pltpu.VMEM((width, cols), BF16),
@@ -290,25 +372,35 @@
             pltpu.VMEM((rows, heads, 2 * hd), F32),
             pltpu.VMEM((rows, heads, hd), F32),
             pltpu.VMEM((rows, cols), F32),
-            pltpu.SemaphoreType.DMA((6,)),
+            pltpu.SemaphoreType.DMA((9,)),
             pltpu.SemaphoreType.DMA((4,)),
         ],
-        compiler_params=pltpu.CompilerParams(vmem_limit_bytes=48 * 1024 * 1024),
+        compiler_params=pltpu.CompilerParams(vmem_limit_bytes=GRANT),
         name="mixer",
     )(
         tokens, lower_bound.reshape(1, cols), head_gain.reshape(1, hd),
         old_state, w_query, w_forget, w_value, w_gate, w_out,
     )
     ff = expert_gate.shape[2]
-    slab = pltpu.VMEM((n, slots, half), BF16)
+    spare = slots - capacity
+    wide = half
+    if spare and capacity % spare == 0 and half % ((capacity // spare + 1) * 128) == 0:
+        wide = half // (capacity // spare + 1) * (capacity // spare)
+    slab = pltpu.VMEM((n, slots, wide), BF16)
     pieces = 4
     dma = pltpu.SemaphoreType.DMA
     next_tokens = pl.pallas_call(
         functools.partial(expert_kernel, capacity, n),
         out_shape=jax.ShapeDtypeStruct((rows, half), BF16),
-        in_specs=[vmem] * 6 + [hbm] * 3,
+        in_specs=[hbm] * 9,
         out_specs=vmem,
         scratch_shapes=[
+            pltpu.VMEM((rows, width), BF16),
+            pltpu.VMEM((rows, width), BF16),
+            pltpu.VMEM((1, width), F32),
+            pltpu.VMEM((top, rows), jnp.int32),
+            pltpu.VMEM((top, rows), F32),
+            pltpu.VMEM((1, width), F32),
             pltpu.VMEM((width, ff), BF16),
             pltpu.VMEM((width, ff), BF16),
             pltpu.VMEM((ff, width), BF16),
@@ -317,15 +409,15 @@
             slab, slab, slab, slab, slab, slab, slab,
             pltpu.VMEM((rows, 128), F32),
             pltpu.VMEM((rows, 128), F32),
-            dma((3,)), dma((4,)), dma((n,)), dma((n,)), dma((n,)), dma((n,)), dma((n,)), dma((n,)),
+            dma((9,)), dma((4,)), dma((n,)), dma((n,)), dma((n,)), dma((n,)), dma((n,)), dma((n,)),
             dma((pieces,)), dma((pieces,)),
         ],
         compiler_params=pltpu.CompilerParams(
-            collective_id=0, has_side_effects=True, vmem_limit_bytes=48 * 1024 * 1024
+            collective_id=0, has_side_effects=True, vmem_limit_bytes=GRANT
         ),
         name="experts",
     )(
-        part, tokens, mix_gain.reshape(1, width), expert_ids, route_weight,
+        part, tokens, mix_gain.reshape(1, width), expert_ids.T, route_weight.T,
         moe_gain.reshape(1, width), expert_gate.reshape(width, ff), expert_up.reshape(width, ff),
         expert_down.reshape(ff, width),
     )

time: 44 us -> 39 us (0.89)
  local copies, waits for them, and re-layouts: 7.57 us -> 1.42 us
  Pallas kernels: 35.5 us -> 36.7 us
    unnamed x23 -> x1, local copies, waits for them, and re-layouts: 7.57 us -> 1.42 us
    pallas_call x1, Pallas kernels: 7.99 us -> 9.2 us  [per_device(): pl.pallas_call(mixer_kernel, out_shape=(jax.ShapeDtypeStruct(old_state.sh...]
where the time goes in v2:
time: 39 us; the launch traced here: 38.8 us
  Pallas kernels  36.7 us (94%)
  local copies, waits for them, and re-layouts  1.42 us (4%)
  between operations  0.65 us (2%)
    pallas_call x1, Pallas kernels, per_device(): pl.pallas_call(functools.partial(expert_kernel, capacity, n), out_shape=j...  27.5 us
    pallas_call x1, Pallas kernels, per_device(): pl.pallas_call(mixer_kernel, out_shape=(jax.ShapeDtypeStruct(old_state.sh...  9.2 us
    unnamed x1, local copies, waits for them, and re-layouts  1.42 us

profile of v2, /device:TPU:0, one launch (start us, length us, event | category | flops | bytes accessed | tf_op | source)
XLA Modules:
  0.0 38.8 jit_solution(3014761403941314106)
XLA Ops:
  0.6 9.2 %mixer.1 = (f32[24,8,4096]{2,1,0:T(8,128)}, bf16[24,2048]{1,0:T(8,128)(2,1)}) custom-call(bf16[24,2048]{1,0:T(8,128)(2,1)} %tok_hbm.3, f32[1,512]{1,0:T(1,128)} %bitcast.14, f32[1,64]{1,0:T(1,128)} %bitcast.17, f32[24,8,4096]{2,1,0:T(8,128)} %st_hbm.1, bf16[2048,512]{1,0:T(8,128)(2,1)} %wq_hbm.1, bf16[2048,512]{1,0:T(8,128)(2,1)} %wf_hbm.1, ...), custom_call_target="tpu_custom_call" | custom-call | tf_op jit(solution)/shard_map/mixer/pallas_call | solution.py:350
  9.8 27.5 %experts.1 = bf16[24,1024]{1,0:T(8,128)(2,1)} custom-call(bf16[24,2048]{1,0:T(8,128)(2,1)} %get-tuple-element.4.part_hbm, bf16[24,2048]{1,0:T(8,128)(2,1)} %tok_hbm.3, f32[1,2048]{1,0:T(1,128)} %bitcast.12, s32[2,24]{1,0:T(2,128)} %bitcast.15, f32[2,24]{1,0:T(2,128)} %bitcast.16, f32[1,2048]{1,0:T(1,128)} %bitcast.13, bf16[2048,256]{1,0:T(8,128)(2,1)} %bitcast.9, ...), custom_call_target="tpu_custom_call" | custom-call | tf_op jit(solution)/shard_map/experts/pallas_call | solution.py:392
  37.4 1.4 %copy.19 = bf16[24,1024]{1,0:T(8,128)(2,1)} copy(bf16[24,1024]{1,0:T(8,128)(2,1)} %experts.1) | data formatting | bytes 98304

commit v3 on v2

--- a/solution.py
+++ b/solution.py
@@ -413,7 +413,7 @@
             dma((pieces,)), dma((pieces,)),
         ],
         compiler_params=pltpu.CompilerParams(
-            collective_id=0, has_side_effects=True, vmem_limit_bytes=GRANT
+            collective_id=0, has_side_effects=True, vmem_limit_bytes=40 * 2**20
         ),
         name="experts",
     )(

time: 39 us -> 42.1 us (1.079)
  local copies, waits for them, and re-layouts: 1.42 us -> 5.2 us
  Pallas kernels: 36.7 us -> 35.9 us
    unnamed x1 -> x19, local copies, waits for them, and re-layouts: 1.42 us -> 5.2 us
    pallas_call x1, Pallas kernels: 27.5 us -> 26.7 us  [per_device(): pl.pallas_call(functools.partial(expert_kernel, capacity, n), out_shape=j...]
where the time goes in v3:
time: 42.1 us; the launch traced here: 41.9 us
  Pallas kernels  35.9 us (85%)
  local copies, waits for them, and re-layouts  5.2 us (12%)
  between operations  0.74 us (2%)
    pallas_call x1, Pallas kernels, per_device(): pl.pallas_call(functools.partial(expert_kernel, capacity, n), out_shape=j...  26.7 us
    pallas_call x1, Pallas kernels, per_device(): pl.pallas_call(mixer_kernel, out_shape=(jax.ShapeDtypeStruct(old_state.sh...  9.26 us
    unnamed x19, local copies, waits for them, and re-layouts  5.2 us

profile of v3, /device:TPU:0, one launch (start us, length us, event | category | flops | bytes accessed | tf_op | source)
XLA Modules:
  0.0 41.9 jit_solution(11948286310276061089)
XLA Ops:
  0.6 0.0 copy-start.3
  0.6 0.0 copy-start.5
  0.7 0.0 copy-start.6
  0.7 0.0 copy-start.7
  0.7 0.0 copy-start.8
  0.7 9.3 %mixer.1 = (f32[24,8,4096]{2,1,0:T(8,128)}, bf16[24,2048]{1,0:T(8,128)(2,1)}) custom-call(bf16[24,2048]{1,0:T(8,128)(2,1)} %tok_hbm.3, f32[1,512]{1,0:T(1,128)} %bitcast.16, f32[1,64]{1,0:T(1,128)} %bitcast.17, f32[24,8,4096]{2,1,0:T(8,128)} %st_hbm.1, bf16[2048,512]{1,0:T(8,128)(2,1)} %wq_hbm.1, bf16[2048,512]{1,0:T(8,128)(2,1)} %wf_hbm.1, ...), custom_call_target="tpu_custom_call" | custom-call | tf_op jit(solution)/shard_map/mixer/pallas_call | solution.py:350
  9.9 0.0 copy-done.3
  10.0 0.0 copy-done.5
  10.0 0.0 copy-done.6
  10.0 0.0 copy-done.7
  10.0 0.0 copy-done.8
  10.0 0.0 copy-start
  10.0 1.2 %copy-done = bf16[1,2048,256]{2,1,0:T(8,128)(2,1)S(1)} copy-done((bf16[1,2048,256]{2,1,0:T(8,128)(2,1)S(1)}, bf16[1,2048,256]{2,1,0:T(8,128)(2,1)}, u32[]{:S(2)}) %copy-start) | copy-done | bytes 1048600
  11.2 0.0 copy-start.1
  11.2 1.2 %copy-done.1 = bf16[1,2048,256]{2,1,0:T(8,128)(2,1)S(1)} copy-done((bf16[1,2048,256]{2,1,0:T(8,128)(2,1)S(1)}, bf16[1,2048,256]{2,1,0:T(8,128)(2,1)}, u32[]{:S(2)}) %copy-start.1) | copy-done | bytes 1048600
  12.5 0.0 copy-start.2
  12.5 1.2 %copy-done.2 = bf16[1,256,2048]{2,1,0:T(8,128)(2,1)S(1)} copy-done((bf16[1,256,2048]{2,1,0:T(8,128)(2,1)S(1)}, bf16[1,256,2048]{2,1,0:T(8,128)(2,1)}, u32[]{:S(2)}) %copy-start.2) | copy-done | bytes 1048600
  13.7 0.0 copy-start.4
  13.7 0.9 %copy-done.4 = bf16[24,2048]{1,0:T(8,128)(2,1)S(1)} copy-done((bf16[24,2048]{1,0:T(8,128)(2,1)S(1)}, bf16[24,2048]{1,0:T(8,128)(2,1)}, u32[]{:S(2)}) %copy-start.4) | copy-done | bytes 98328
  14.6 26.7 %experts.1 = bf16[24,1024]{1,0:T(8,128)(2,1)S(1)} custom-call(bf16[24,2048]{1,0:T(8,128)(2,1)S(1)} %copy-done.4, bf16[24,2048]{1,0:T(8,128)(2,1)S(1)} %copy-done.3, f32[1,2048]{1,0:T(1,128)S(1)} %bitcast.12, s32[2,24]{1,0:T(2,128)S(1)} %bitcast.14, f32[2,24]{1,0:T(2,128)S(1)} %bitcast.15, f32[1,2048]{1,0:T(1,128)S(1)} %bitcast.13, ...), custom_call_target="tpu_custom_call" | custom-call | tf_op jit(solution)/shard_map/experts/pallas_call | solution.py:392
  41.2 0.6 %copy.19 = bf16[24,1024]{1,0:T(8,128)(2,1)} copy(bf16[24,1024]{1,0:T(8,128)(2,1)S(1)} %experts.1) | data formatting | bytes 98304
Async XLA Ops:
  0.6 9.3 %copy-start.3 = (bf16[24,2048]{1,0:T(8,128)(2,1)S(1)}, bf16[24,2048]{1,0:T(8,128)(2,1)}, u32[]{:S(2)}) copy-start(bf16[24,2048]{1,0:T(8,128)(2,1)} %tok_hbm.3) | copy-start | bytes 294916
  0.6 9.3 %copy-start.5 = (f32[2048]{0:T(1024)S(1)}, f32[2048]{0:T(1024)}, u32[]{:S(2)}) copy-start(f32[2048]{0:T(1024)} %param.25) | copy-start | bytes 24580
  0.7 9.3 %copy-start.6 = (f32[2048]{0:T(1024)S(1)}, f32[2048]{0:T(1024)}, u32[]{:S(2)}) copy-start(f32[2048]{0:T(1024)} %param.31) | copy-start | bytes 24580
  0.7 9.3 %copy-start.7 = (s32[24,2]{0,1:T(2,128)S(1)}, s32[24,2]{0,1:T(2,128)}, u32[]{:S(2)}) copy-start(s32[24,2]{0,1:T(2,128)} %param.29) | copy-start | bytes 580
  0.7 9.3 %copy-start.8 = (f32[24,2]{0,1:T(2,128)S(1)}, f32[24,2]{0,1:T(2,128)}, u32[]{:S(2)}) copy-start(f32[24,2]{0,1:T(2,128)} %param.30) | copy-start | bytes 580
  10.0 1.2 %copy-start = (bf16[1,2048,256]{2,1,0:T(8,128)(2,1)S(1)}, bf16[1,2048,256]{2,1,0:T(8,128)(2,1)}, u32[]{:S(2)}) copy-start(bf16[1,2048,256]{2,1,0:T(8,128)(2,1)} %param.26) | copy-start | bytes 3145732
  11.2 1.2 %copy-start.1 = (bf16[1,2048,256]{2,1,0:T(8,128)(2,1)S(1)}, bf16[1,2048,256]{2,1,0:T(8,128)(2,1)}, u32[]{:S(2)}) copy-start(bf16[1,2048,256]{2,1,0:T(8,128)(2,1)} %param.27) | copy-start | bytes 3145732
  12.5 1.2 %copy-start.2 = (bf16[1,256,2048]{2,1,0:T(8,128)(2,1)S(1)}, bf16[1,256,2048]{2,1,0:T(8,128)(2,1)}, u32[]{:S(2)}) copy-start(bf16[1,256,2048]{2,1,0:T(8,128)(2,1)} %param.28) | copy-start | bytes 3145732
  13.7 0.9 %copy-start.4 = (bf16[24,2048]{1,0:T(8,128)(2,1)S(1)}, bf16[24,2048]{1,0:T(8,128)(2,1)}, u32[]{:S(2)}) copy-start(bf16[24,2048]{1,0:T(8,128)(2,1)} %get-tuple-element.4.part_hbm) | copy-start | bytes 294916
